TPU v7x, 32 devices: a whole 2x2x4 slice. The times are simulated.
32 devices in a mesh: grp: 2 (over y), sp: 4 (over z), tp: 4 (over x, core).
Axes of the slice: x: 2, y: 2, z: 4, core: 2. Of those that a mesh axis runs over, the one named last changes fastest.
Arguments:
- stream: bfloat16 [2048, 4096], P(('grp', 'sp'), 'tp'), parts along dimension 0, may hold values from -6 to 6
- gain_pre: float32 [3, 4096], replicated, may hold values from 0.1 to 1.9
- w_in: bfloat16 [3, 4096, 1024], P(None, 'sp', 'tp'), may hold values from -0.09375 to 0.09375
- w_pool: bfloat16 [3, 4, 256, 256], P(None, 'tp'), may hold values from -0.375 to 0.375
- pool_scale: float32 [3, 1024], P(None, 'tp'), may hold values from 0.1 to 1.9
- w_out: bfloat16 [3, 1024, 4096], P(None, 'tp', 'sp'), may hold values from -0.5 to 0.5
- gain_post: float32 [3, 4096], replicated, may hold values from 0.1 to 1.9
Outputs:
- result: bfloat16 [2048, 4096], P(('grp', 'sp'), 'tp'), parts along dimension 0
There are 2 independent parts, one for each index of `grp`. A program takes and returns all parts, laid end to end along the dimension named above; an argument that names none is the same for every part. Nothing has to cross between parts.
All inputs are finite; a program needn't handle non-finite values.
Results may differ from a plain program's by a relative error of at most 0.02.
Values may be sent and summed in bfloat16 or wider, within the bound.
A program may use at most 64 MiB of HBM per device.

v0:
```python
import functools

import jax
import jax.numpy as jnp
from jax import lax
from jax.experimental import pallas as pl
from jax.experimental.pallas import tpu as pltpu
from jax.sharding import PartitionSpec as P

EPS = 1e-06
HALO = 16
CHUNKS = 4
PIECES = 2
MESH = pl.DeviceIdType.MESH
F32 = jnp.float32
BF16 = jnp.bfloat16


def kernel(
    G, S, T, layers, width,
    stream, gain_pre, w_in, w_pool, pool_scale, w_out, gain_post,
    out,
    win, wout, ag, part, pair, summed, xgot, normed, acc, ss, scale, branch, ext, halo, sq,
    load_sem, zs_sem, zr_sem, ys_sem, yr_sem,
    agp_sem, agx_sem, agr_sem, ps_sem, pr_sem, xs_sem, xr_sem, qs_sem, qr_sem, hs_sem, hr_sem,
):
    g, s, t = lax.axis_index("grp"), lax.axis_index("sp"), lax.axis_index("tp")
    pairs = T // 2
    p, c = lax.div(t, 2), lax.rem(t, 2)
    mate = p * 2 + 1 - c
    R, F = stream.shape
    group = w_pool.shape[2]
    rows_in, cols_out = w_in.shape[1], w_out.shape[2]
    per = S // T
    use_y = G == 2

    def remote(src, dst, send, recv, where):
        return pltpu.make_async_remote_copy(
            src_ref=src, dst_ref=dst, send_sem=send, recv_sem=recv,
            device_id=where, device_id_type=MESH,
        )

    def span(m, src, h):
        size = rows_in if m % 2 == 0 else group
        share = size // 2 if use_y else size
        length = share // PIECES
        start = (g * share if use_y else 0) + h * length
        if m % 2 == 0:
            return win.at[m // 2, pl.ds(pl.multiple_of(src * size + start, 16), length), :]
        return wout.at[m // 2, src, pl.ds(pl.multiple_of(start, 16), length), :]

    def z_copy(m, src, way, h):
        view = span(m, src, h)
        to = s + 1 if way == 0 else s - 1
        return remote(view, view, zs_sem.at[m, src, way, h], zr_sem.at[m, src, h], {"sp": to})

    def y_copy(m, src, h):
        view = span(m, src, h)
        return remote(view, view, ys_sem.at[m, src, h], yr_sem.at[m, src, h], {"grp": 1 - g})

    def load(m):
        if m % 2 == 0:
            return pltpu.make_async_copy(
                w_in.at[m // 2],
                win.at[m // 2, pl.ds(pl.multiple_of(s * rows_in, 16), rows_in), :],
                load_sem.at[m],
            )
        return pltpu.make_async_copy(w_out.at[m // 2], wout.at[m // 2, s], load_sem.at[m])

    M = 2 * layers

    def own(m):
        if m < M:
            load(m).wait()
            for h in range(PIECES):
                pl.when(s < S - 1)(lambda: z_copy(m, s, 0, h).start())
                pl.when(s > 0)(lambda: z_copy(m, s, 1, h).start())

    def relay(m, k, h):
        def from_left():
            src = s - 1 - k
            z_copy(m, src, 0, h).wait_recv()
            pl.when(s < S - 1)(lambda: z_copy(m, src, 0, h).start())
            if use_y:
                y_copy(m, src, h).start()

        def from_right():
            src = s + 1 + k
            z_copy(m, src, 1, h).wait_recv()
            pl.when(s > 0)(lambda: z_copy(m, src, 1, h).start())
            if use_y:
                y_copy(m, src, h).start()

        pl.when(s - 1 - k >= 0)(from_left)
        pl.when(s + 1 + k <= S - 1)(from_right)

    units = [(m, k, h) for m in range(M) for k in range(S - 1) for h in range(PIECES)]
    done = [0]

    def tick(n=1):
        for mm, k, h in units[done[0] : done[0] + n]:
            relay(mm, k, h)
            if k == min(1, S - 2) and h == PIECES - 1:
                own(mm + 1)
            done[0] += 1

    def pump(m):
        tick(max(0, (m + 1) * (S - 1) * PIECES - done[0]))

    def finish(m):
        if use_y:
            for src in range(S):
                for h in range(PIECES):
                    pl.when(s != src)(lambda: y_copy(m, src, h).wait_recv())

    def cut(l):
        return R // 2 - HALO * (layers - 1) + HALO * l

    def span_in(l, a):
        return (cut(l), R) if a == 0 else (0, cut(l))

    def span_out(l, a):
        return span_in(l + 1, a)

    def bits(bounds):
        lo, hi = bounds
        mid = lo + ((hi - lo) // 2 + 15) // 16 * 16
        return [(lo, mid), (mid, hi)]

    def sweep(bounds, body):
        lo, hi = bounds
        step = 32 if (hi - lo) % 32 == 0 else 16

        def one(i, carry):
            body(pl.ds(pl.multiple_of(lo + i * step, 16), step))
            return carry

        lax.fori_loop(0, (hi - lo) // step, one, 0)

    def lanes(x):
        return sum(x[:, i : i + 128] for i in range(0, F, 128))

    def ag_copy(l, block, a, i, sem, to):
        lo, hi = bits(span_in(l, a))[i]
        view = ag.at[l, block, pl.ds(lo, hi - lo), :]
        n = a * 2 + i
        return remote(view, view, sem, agr_sem.at[l, block, n], {"tp": to})

    def ag_start(l, a):
        for i in range(2):
            n = a * 2 + i
            for d in range(1, pairs):
                q = lax.rem(p + d, pairs)
                ag_copy(l, t, a, i, agx_sem.at[l, q, n], q * 2 + c).start()
        for i in range(2):
            ag_copy(l, t, a, i, agp_sem.at[l, p, a * 2 + i], mate).start()

    def ag_wait(l, block, a):
        for i in range(2):
            ag_copy(l, block, a, i, agp_sem.at[l, p, a * 2 + i], mate).wait_recv()

    def ag_relay(l, a):
        for d in range(1, pairs):
            q = lax.rem(p + d, pairs)
            for i in range(2):
                copy = ag_copy(l, q * 2 + c, a, i, agp_sem.at[l, q, a * 2 + i], mate)
                copy.wait_recv()
                copy.start()

    def absorb(l, block, a, first):
        lo, hi = span_in(l, a)
        gain = gain_pre[pl.ds(l, 1), pl.ds(pl.multiple_of(block * F, 128), F)]

        def body(rows):
            x = ag[l, block, rows, :].astype(F32)
            square = lanes(x * x)
            ss[rows, :] = square if first else ss[rows, :] + square
            normed[rows, :] = (x * gain).astype(BF16)

        sweep((lo, hi), body)
        product = jnp.dot(
            normed[lo:hi, :], win[l, pl.ds(pl.multiple_of(block * F, 128), F), :],
            preferred_element_type=F32,
        )
        acc[lo:hi, :] = product if first else acc[lo:hi, :] + product

    def inner(l, a):
        lo, hi = span_in(l, a)
        absorb(l, t, a, True)
        ag_wait(l, mate, a)
        absorb(l, mate, a, False)
        for d in range(1, pairs):
            q = lax.rem(p + d, pairs)
            absorb(l, q * 2 + c, a, False)
            ag_wait(l, q * 2 + 1 - c, a)
            absorb(l, q * 2 + 1 - c, a, False)
        inverse = lax.rsqrt(jnp.sum(ss[lo:hi, :], axis=1, keepdims=True) / width + EPS)
        ext[l, HALO + lo : HALO + hi, :] = (acc[lo:hi, :] * inverse).astype(BF16)

    def halo_copy(l):
        return remote(
            ext.at[l, pl.ds(R, HALO), :], halo.at[l], hs_sem.at[l], hr_sem.at[l], {"sp": s + 1}
        )

    def halo_in(l):
        pl.when(s > 0)(lambda: halo_copy(l).wait_recv())

        @pl.when(s == 0)
        def _():
            ext[l, pl.ds(0, HALO), :] = jnp.zeros((HALO, group), BF16)

        @pl.when(s > 0)
        def _():
            ext[l, pl.ds(0, HALO), :] = halo[l]

    def pool(l, a):
        lo, hi = span_out(l, a)
        values = ext[l, lo : hi + HALO, :].astype(F32)
        two = values + pltpu.roll(values, 1, 0)
        four = two + pltpu.roll(two, 2, 0)
        eight = four + pltpu.roll(four, 4, 0)
        sixteen = eight + pltpu.roll(eight, 8, 0)
        total = jnp.where(t == 0, two, jnp.where(t == 1, four, jnp.where(t == 2, eight, sixteen)))
        window = jnp.where(t == 0, 2, jnp.where(t == 1, 4, jnp.where(t == 2, 8, 16)))
        place = s * R + lo + lax.broadcasted_iota(jnp.int32, (hi - lo, group), 0)
        count = jnp.minimum(place + 1, window).astype(F32)
        spread = (total[HALO:, :] / count - values[HALO:, :]).astype(BF16)
        mixed = jnp.dot(spread, w_pool[l, 0], preferred_element_type=F32)
        return (mixed * pool_scale[l : l + 1, :]).astype(BF16)

    def project(l, a, dest, mixed):
        lo, hi = span_out(l, a)
        for k in range(per):
            value = jnp.dot(mixed, wout[l, dest * per + k], preferred_element_type=F32)
            part[l, dest, lo:hi, k * cols_out : (k + 1) * cols_out] = value.astype(BF16)

    def pair_copy(l, q, a, i):
        lo, hi = bits(span_out(l, a))[i]
        rows, n = pl.ds(lo, hi - lo), a * 2 + i
        return remote(
            part.at[l, q * 2 + 1 - c, rows, :], pair.at[l, q, rows, :],
            ps_sem.at[l, q, n], pr_sem.at[l, q, n], {"tp": mate},
        )

    def cross_copy(l, q, slot, a, i):
        lo, hi = bits(span_out(l, a))[i]
        rows, n = pl.ds(lo, hi - lo), a * 2 + i
        return remote(
            summed.at[l, q, rows, :], xgot.at[l, slot, rows, :],
            xs_sem.at[l, q, n], xr_sem.at[l, slot, n], {"tp": q * 2 + c},
        )

    def scatter_first(l, a, mixed):
        for d in range(1, pairs):
            q = lax.rem(p + d, pairs)
            project(l, a, q * 2 + 1 - c, mixed)
            for i in range(2):
                pair_copy(l, q, a, i).start()
        for d in range(1, pairs):
            project(l, a, lax.rem(p + d, pairs) * 2 + c, mixed)

    def scatter_cross(l, a):
        for d in range(1, pairs):
            q = lax.rem(p + d, pairs)
            for i in range(2):
                pair_copy(l, q, a, i).wait_recv()

                def body(rows):
                    summed[l, q, rows, :] = (
                        part[l, q * 2 + c, rows, :].astype(F32) + pair[l, q, rows, :].astype(F32)
                    ).astype(BF16)

                sweep(bits(span_out(l, a))[i], body)
                cross_copy(l, q, p, a, i).start()

    def scatter_own(l, a, mixed):
        project(l, a, mate, mixed)
        for i in range(2):
            pair_copy(l, p, a, i).start()
        project(l, a, t, mixed)

    def sq_copy(l, slot, a, to):
        view = sq.at[l, a, slot]
        return remote(view, view, qs_sem.at[l, a, to], qr_sem.at[l, a, slot], {"tp": to})

    def settle(l, a):
        for i in range(2):
            pair_copy(l, p, a, i).wait_recv()
            for d in range(1, pairs):
                q = lax.rem(p + d, pairs)
                cross_copy(l, q, q, a, i).wait_recv()

            def add(rows):
                value = part[l, t, rows, :].astype(F32) + pair[l, p, rows, :].astype(F32)
                for d in range(1, pairs):
                    value = value + xgot[l, lax.rem(p + d, pairs), rows, :].astype(F32)
                branch[rows, :] = value
                ss[rows, :] = lanes(value * value)

            sweep(bits(span_out(l, a))[i], add)
        row = jnp.sum(jnp.transpose(ss[...]), axis=0, keepdims=True)
        sq[l, a, t] = jnp.broadcast_to(row, (8, R))
        for d in range(1, T):
            sq_copy(l, t, a, lax.rem(t + d, T)).start()
        tick()
        for d in range(1, T):
            other = lax.rem(t + d, T)
            sq_copy(l, other, a, other).wait_recv()
        squares = sq[l, a, 0]
        for k in range(1, T):
            squares = squares + sq[l, a, k]
        inverse = lax.rsqrt(squares / width + EPS)
        scale[...] = jnp.transpose(jnp.concatenate([inverse] * 16, axis=0))
        gain = gain_post[pl.ds(l, 1), pl.ds(pl.multiple_of(t * F, 128), F)]

        def update(rows):
            value = ag[l, t, rows, :].astype(F32) + branch[rows, :] * scale[rows, 0:1] * gain
            if l + 1 < layers:
                ag[l + 1, t, rows, :] = value.astype(BF16)
            else:
                out[rows, :] = value.astype(BF16)

        sweep(span_out(l, a), update)
        if l + 1 < layers:
            ag_start(l + 1, a)

    for m in range(M):
        load(m).start()
    barrier = pltpu.get_barrier_semaphore()

    def greet(where):
        pl.semaphore_signal(barrier, inc=1, device_id=where, device_id_type=MESH)

    pl.when(s < S - 1)(lambda: greet({"sp": s + 1}))
    pl.when(s > 0)(lambda: greet({"sp": s - 1}))
    if use_y:
        greet({"grp": 1 - g})
    for d in range(1, T):
        greet({"tp": lax.rem(t + d, T)})
    ag[0, t] = stream[...]
    ends = jnp.where(s > 0, 1, 0) + jnp.where(s < S - 1, 1, 0)
    pl.semaphore_wait(barrier, ends + (1 if use_y else 0) + T - 1)

    own(0)
    ag_start(0, 0)
    ag_start(0, 1)
    each = (S - 1) * PIECES
    for l in range(layers):
        if l == 0:
            tick(each // 3)
            ag_relay(0, 0)
            tick(each // 3)
            ag_relay(0, 1)
        else:
            ag_relay(l, 0)
        pump(2 * l)
        finish(2 * l)
        inner(l, 0)
        pl.when(s < S - 1)(lambda: halo_copy(l).start())
        mixed = pool(l, 0)
        if l == 0:
            tick()
            inner(l, 1)
            tick()
            halo_in(l)
            later = pool(l, 1)
        pump(2 * l + 1)
        finish(2 * l + 1)
        scatter_first(l, 0, mixed)
        tick()
        if l > 0:
            ag_relay(l, 1)
        scatter_cross(l, 0)
        tick()
        scatter_own(l, 0, mixed)
        tick()
        if l > 0:
            inner(l, 1)
            tick()
            halo_in(l)
            later = pool(l, 1)
        scatter_first(l, 1, later)
        tick()
        scatter_cross(l, 1)
        tick()
        scatter_own(l, 1, later)
        tick()
        settle(l, 0)
        tick()
        settle(l, 1)
        tick()

    for l in range(layers):
        pl.when(s < S - 1)(lambda: halo_copy(l).wait_send())
        for a in range(2):
            for d in range(1, T):
                sq_copy(l, t, a, lax.rem(t + d, T)).wait_send()
            for i in range(2):
                n = a * 2 + i
                for q in range(pairs):
                    ag_copy(l, t, a, i, agp_sem.at[l, q, n], mate).wait_send()
                    pair_copy(l, q, a, i).wait_send()
                for d in range(1, pairs):
                    q = lax.rem(p + d, pairs)
                    ag_copy(l, t, a, i, agx_sem.at[l, q, n], mate).wait_send()
                    cross_copy(l, q, p, a, i).wait_send()
    for m in range(M):
        for src in range(S):
            for h in range(PIECES):
                pl.when(jnp.logical_and(src <= s, s < S - 1))(lambda: z_copy(m, src, 0, h).wait_send())
                pl.when(jnp.logical_and(src >= s, s > 0))(lambda: z_copy(m, src, 1, h).wait_send())
                if use_y:
                    pl.when(s != src)(lambda: y_copy(m, src, h).wait_send())


def per_device(G, S, T, stream, gain_pre, w_in, w_pool, pool_scale, w_out, gain_post):
    layers, width = gain_pre.shape
    R, F = stream.shape
    group = w_pool.shape[2]
    pairs = T // 2
    M = 2 * layers
    dma = pltpu.SemaphoreType.DMA
    vmem = pl.BlockSpec(memory_space=pltpu.VMEM)
    anywhere = pl.BlockSpec(memory_space=pl.ANY)
    return pl.pallas_call(
        functools.partial(kernel, G, S, T, layers, width),
        out_shape=jax.ShapeDtypeStruct((R, F), BF16),
        in_specs=[vmem, vmem, anywhere, vmem, vmem, anywhere, vmem],
        out_specs=vmem,
        scratch_shapes=[
            pltpu.VMEM((layers, width, group), BF16),
            pltpu.VMEM((layers, S, group, w_out.shape[2]), BF16),
            pltpu.VMEM((layers, T, R, F), BF16),
            pltpu.VMEM((layers, T, R, F), BF16),
            pltpu.VMEM((layers, pairs, R, F), BF16),
            pltpu.VMEM((layers, pairs, R, F), BF16),
            pltpu.VMEM((layers, pairs, R, F), BF16),
            pltpu.VMEM((R, F), BF16),
            pltpu.VMEM((R, group), F32),
            pltpu.VMEM((R, 128), F32),
            pltpu.VMEM((R, 128), F32),
            pltpu.VMEM((R, F), F32),
            pltpu.VMEM((layers, HALO + R, group), BF16),
            pltpu.VMEM((layers, HALO, group), BF16),
            pltpu.VMEM((layers, 2, T, 8, R), F32),
            dma((M,)),
            dma((M, S, 2, PIECES)),
            dma((M, S, PIECES)),
            dma((M, S, PIECES)),
            dma((M, S, PIECES)),
            dma((layers, pairs, CHUNKS)),
            dma((layers, pairs, CHUNKS)),
            dma((layers, T, CHUNKS)),
            dma((layers, pairs, CHUNKS)),
            dma((layers, pairs, CHUNKS)),
            dma((layers, pairs, CHUNKS)),
            dma((layers, pairs, CHUNKS)),
            dma((layers, 2, T)),
            dma((layers, 2, T)),
            dma((layers,)),
            dma((layers,)),
        ],
        compiler_params=pltpu.CompilerParams(
            collective_id=0, has_side_effects=True, vmem_limit_bytes=60 * 1024 * 1024
        ),
    )(stream, gain_pre, w_in, w_pool, pool_scale, w_out, gain_post)


def solution(mesh):
    G, S, T = mesh.shape["grp"], mesh.shape["sp"], mesh.shape["tp"]
    return jax.shard_map(
        functools.partial(per_device, G, S, T),
        mesh=mesh,
        in_specs=(
            P(("grp", "sp"), "tp"),
            P(),
            P(None, "sp", "tp"),
            P(None, "tp", None, None),
            P(None, "tp"),
            P(None, "tp", "sp"),
            P(),
        ),
        out_specs=P(("grp", "sp"), "tp"),
        check_vma=False,
    )
```

profile of v0, /device:TPU:25, one launch (start us, length us, event | category | flops | bytes accessed | tf_op | source)
XLA Modules:
  0.0 143.0 jit_solution(13568392885194236190)
XLA Ops:
  0.0 141.2 %shard_map.73 = bf16[256,1024]{1,0:T(8,128)(2,1)} custom-call(bf16[256,1024]{1,0:T(8,128)(2,1)} %stream.1, f32[3,4096]{1,0:T(4,128)} %gain_pre.1, bf16[3,1024,256]{2,1,0:T(8,128)(2,1)} %w_in.1, bf16[3,1,256,256]{3,2,1,0:T(8,128)(2,1)} %w_pool.1, f32[3,256]{1,0:T(4,128)} %pool_scale.1, bf16[3,256,1024]{2,1,0:T(8,128)(2,1)} %w_out.1, f32[3,4096]{1,0:T(4,128)} %gain_post.1), custom_call_target="tpu_custom_call" | custom-call | tf_op jit(solution)/shard_map/pallas_call | solution.py:425
  141.2 1.9 %copy.9 = bf16[256,1024]{1,0:T(8,128)(2,1)} copy(bf16[256,1024]{1,0:T(8,128)(2,1)} %shard_map.73) | data formatting | bytes 1048576
where the time goes:
time: 146 us; the launch traced here: 143 us
  Pallas kernels  141 us (97%)
  local copies, waits for them, and re-layouts  1.87 us (1%)
    pallas_call x1, Pallas kernels, per_device(): pl.pallas_call(functools.partial(kernel, G, S, T, layers, width), out_sha...  141 us

commit v1 on v0

--- a/solution.py
+++ b/solution.py
@@ -11,6 +11,10 @@
 HALO = 16
 CHUNKS = 4
 PIECES = 2
+PARTS = 4
+PERIOD, STRIDE = 18, 2
+AT_S, AT_B, AT_C, AT_F, AT_G, AT_D = 2.6, 6, 8, 10.3, 10.8, 13.5
+LEAD, SPACE, RELAY, SECOND = 17.9, 1.5, 8, 4
 MESH = pl.DeviceIdType.MESH
 F32 = jnp.float32
 BF16 = jnp.bfloat16
@@ -466,10 +470,610 @@
     )(stream, gain_pre, w_in, w_pool, pool_scale, w_out, gain_post)
 
 
+def plane_kernel(
+    G, S, T, layers, width, order,
+    stream_hbm, gain_pre_hbm, w_in, w_pool, scale_hbm, w_out, gain_post_hbm,
+    out,
+    stream, gain_pre, gain_post, win, wout, wp, scales, rows_in, x,
+    part, got, far, psq, ext, mix, branch, bsq,
+    load_sem, small_sem, self_sem, y_send, y_recv, x_send, x_recv, f_send, f_recv,
+    wo_send, wo_recv, wx_send, wx_recv, wy_send, wy_recv, wf_send, wf_recv,
+    p_send, p_recv, c_send, c_recv,
+    r_send, r_recv, o_send, o_recv, rq_send, rq_recv, h_send, h_recv, m_send, m_recv, mq_send, mq_recv,
+):
+    g, s, t = lax.axis_index("grp"), lax.axis_index("sp"), lax.axis_index("tp")
+    pairs = T // 2
+    p, c = lax.div(t, 2), lax.rem(t, 2)
+    mate = p * 2 + 1 - c
+    R, F = stream.shape
+    C = R // T
+    group = w_pool.shape[2]
+    sides = 2 if G == 2 else 1
+    side = g if sides == 2 else 0
+    M = 2 * layers
+    line_width = psq.shape[-1]
+    H = S // 2
+    low = lax.div(s, H) * H
+    here = s - low
+    hub, far_hub = jnp.where(low == 0, H - 1, H), jnp.where(low == 0, H, H - 1)
+    is_hub = s == hub
+    near = [low + lax.rem(here + d, H) for d in range(1, H)]
+    away = [H - low + d for d in range(H)]
+    planes = near + away
+
+    def slot(k):
+        return lax.rem(k - low + S, S)
+
+    def remote(src, dst, send, recv, where):
+        return pltpu.make_async_remote_copy(
+            src_ref=src, dst_ref=dst, send_sem=send, recv_sem=recv,
+            device_id=where, device_id_type=MESH,
+        )
+
+    def sent(view, sem):
+        remote(view, view, sem, sem, {"tp": mate}).wait_send()
+
+    def landed(view, sem):
+        remote(view, view, sem, sem, {"tp": mate}).wait_recv()
+
+    barrier = pltpu.get_barrier_semaphore()
+
+    def greet(where):
+        pl.semaphore_signal(barrier, inc=1, device_id=where, device_id_type=MESH)
+
+    for ds in range(S):
+        for dt in range(T):
+            if ds or dt:
+                greet({"sp": lax.rem(s + ds, S), "tp": lax.rem(t + dt, T)})
+    if sides == 2:
+        greet({"grp": 1 - g})
+
+    smalls = [
+        pltpu.make_async_copy(stream_hbm, stream, small_sem.at[0]),
+        pltpu.make_async_copy(gain_pre_hbm, gain_pre, small_sem.at[1]),
+        pltpu.make_async_copy(gain_post_hbm, gain_post, small_sem.at[2]),
+    ]
+    scale_load = pltpu.make_async_copy(scale_hbm, scales, small_sem.at[3])
+
+    def block(m, k):
+        if m % 2 == 0:
+            return win.at[m // 2, slot(k)]
+        return wout.at[m // 2, pl.ds(pl.multiple_of(slot(k) * group, 16), group), :]
+
+    def piece(m, k, half, h):
+        rows = (F if m % 2 == 0 else group) // sides
+        length = rows // PARTS
+        start = half * rows + h * length
+        if m % 2 == 0:
+            return win.at[m // 2, slot(k), pl.ds(pl.multiple_of(start, 16), length), :]
+        return wout.at[m // 2, pl.ds(pl.multiple_of(slot(k) * group + start, 16), length), :]
+
+    def load(m):
+        return pltpu.make_async_copy((w_out if m % 2 else w_in).at[m // 2], block(m, t), load_sem.at[m])
+
+    def own_copy(m, k):
+        return remote(block(m, k), block(m, k), wo_send.at[m], wo_recv.at[m], {"tp": mate})
+
+    def cross_copy(m, k, d, q, h):
+        view = piece(m, k, side, h)
+        return remote(view, view, wx_send.at[m, d], wx_recv.at[m, d, h], {"tp": q * 2 + c})
+
+    def grp_copy(m, d, q, half, h):
+        view = piece(m, q * 2 + c, half, h)
+        return remote(view, view, wy_send.at[m, d], wy_recv.at[m, d, h], {"grp": 1 - g})
+
+    def mate_copy(m, d, q, half, h):
+        view = piece(m, q * 2 + c, half, h)
+        return remote(view, view, wf_send.at[m, d], wf_recv.at[m, d], {"tp": mate})
+
+    others = [(d, lax.rem(p + 1 + d, pairs)) for d in range(pairs - 1)]
+
+    def weight_own(m):
+        load(m).wait()
+        own_copy(m, t).start()
+
+    def weight_cross(m, h):
+        for d, q in others:
+            back = pairs - 2 - d
+            view = piece(m, t, side, h)
+            remote(view, view, wx_send.at[m, d], wx_recv.at[m, back, h], {"tp": q * 2 + c}).start()
+
+    def weight_relay(m, h):
+        for d, q in others:
+            cross_copy(m, q * 2 + c, d, q, h).wait_recv()
+            if sides == 2:
+                grp_copy(m, d, q, side, h).start()
+            mate_copy(m, d, q, side, h).start()
+
+    def weight_second(m, h):
+        if sides == 2:
+            for d, q in others:
+                grp_copy(m, d, q, 1 - side, h).wait_recv()
+                mate_copy(m, d, q, 1 - side, h).start()
+
+    def weight_last(m):
+        for d, q in others:
+            landed(block(m, q * 2 + 1 - c), wf_recv.at[m, d])
+
+    def share(m, k):
+        rows = (F if m % 2 == 0 else group) // sides
+        if m % 2 == 0:
+            return win.at[m // 2, slot(k), pl.ds(0, rows), :]
+        return wout.at[m // 2, pl.ds(pl.multiple_of(slot(k) * group, 16), rows), :]
+
+    def pool_copy(l, d):
+        return remote(wp.at[l], wp.at[l], p_send.at[d - 1], p_recv.at[l], {"tp": lax.rem(t + d, T)})
+
+    def scale_copy(d):
+        return remote(scales, scales, c_send.at[d - 1], c_recv, {"tp": lax.rem(t + d, T)})
+
+    def pool_send(l):
+        @pl.when(t == s)
+        def _():
+            for d in range(1, T):
+                pool_copy(l, d).start()
+
+    def lanes(v):
+        return sum(v[:, i : i + 128] for i in range(0, F, 128))
+
+    def line(square):
+        if C < line_width:
+            square = jnp.concatenate([square, jnp.zeros((line_width - C, 128), F32)], axis=0)
+        row = jnp.sum(jnp.transpose(square), axis=0, keepdims=True)
+        return jnp.broadcast_to(row, (8, line_width))
+
+    def column(values):
+        return jnp.transpose(jnp.concatenate([values] * 16, axis=0))[:C]
+
+    def wide(values, n):
+        return jnp.concatenate([values] * (n // 128), axis=1)
+
+    def squares_start(ref, l, q, send, recv):
+        for d in range(1, S):
+            remote(ref.at[l, q, 0], ref.at[l, q, d], send, recv.at[l, q], {"sp": lax.rem(s + d, S)}).start()
+
+    def squares_wait(ref, l, q, recv):
+        landed(ref.at[l, q, pl.ds(1, S - 1)], recv.at[l, q])
+
+    def total(ref, l, q):
+        return sum(ref[l, q, k] for k in range(S))
+
+    def halo_copy(l, q):
+        ahead = q + lax.div(t + 1, T)
+        return remote(
+            ext.at[l, q, pl.ds(C, HALO), :], ext.at[l, ahead, pl.ds(0, HALO), :],
+            h_send.at[1 if q + 1 == S else 0], h_recv.at[l, ahead], {"tp": lax.rem(t + 1, T)},
+        )
+
+    def run_copy(to, origin):
+        rows = pl.ds(pl.multiple_of(to * C, 16), C)
+        return remote(stream.at[rows, :], rows_in.at[origin], y_send, y_recv.at[origin], {"tp": to})
+
+    def run_of(f, local):
+        return stream.at[pl.ds(pl.multiple_of(t * C, 16), C), :] if local else rows_in.at[f]
+
+    def stream_self(local):
+        return pltpu.make_async_copy(run_of(s, local), x.at[s], self_sem.at[0])
+
+    def stream_on(f, local=False):
+        pl.when(f == s)(lambda: stream_self(local).start())
+        pl.when(f != s)(
+            lambda: remote(run_of(f, local), x.at[s], x_send, x_recv.at[s], {"sp": f}).start()
+        )
+
+    def final_copy(q):
+        rows = pl.ds(pl.multiple_of(t * C, 16), C)
+        return remote(x.at[q], out.at[rows, :], f_send, f_recv, {"sp": q, "tp": s})
+
+    def final_self(q):
+        rows = pl.ds(pl.multiple_of(t * C, 16), C)
+        return pltpu.make_async_copy(x.at[q], out.at[rows, :], self_sem.at[1])
+
+    def features(ref, l):
+        return ref[pl.ds(l, 1), pl.ds(pl.multiple_of(s * F, 128), F)]
+
+    def stage_a(l, q):
+        with jax.named_scope(f"a{l}{q}"):
+            advance(l, q)
+
+    def advance(l, q):
+        if l == 0:
+            pl.when(s == q)(lambda: stream_self(False).wait())
+            pl.when(s != q)(lambda: landed(x.at[q], x_recv.at[q]))
+            value = x[q].astype(F32)
+        else:
+            squares_wait(bsq, l - 1, q, mq_recv)
+            inverse = column(lax.rsqrt(total(bsq, l - 1, q) / width + EPS))
+            new = x[q].astype(F32) + branch[q] * wide(inverse, F) * features(gain_post, l - 1)
+            new = new.astype(BF16)
+            x[q] = new
+            if l == layers:
+                mine = jnp.logical_and(s == q, t == s)
+                pl.when(mine)(lambda: final_self(q).start())
+                pl.when(jnp.logical_not(mine))(lambda: final_copy(q).start())
+                return
+            value = new.astype(F32)
+        psq[l, q, 0] = line(lanes(value * value))
+        squares_start(psq, l, q, rq_send, rq_recv)
+        scaled = (value * features(gain_pre, l)).astype(BF16)
+
+        def project(k):
+            part[l, q, k] = jnp.dot(scaled, win[l, k], preferred_element_type=F32).astype(BF16)
+
+        if q == 0 and l == 0:
+            project(slot(t))
+            landed(block(0, mate), wo_recv.at[0])
+            project(slot(mate))
+            for h in range(PARTS):
+                weight_relay(0, h)
+            for h in range(PARTS):
+                weight_second(0, h)
+            for _, d in others:
+                project(slot(d * 2 + c))
+            weight_last(0)
+            for _, d in others:
+                project(slot(d * 2 + 1 - c))
+            outward(l, q)
+            inward(l, q)
+        else:
+            if q == 0:
+                ready(2 * l)
+            for k in range(H, S):
+                project(k)
+            outward(l, q)
+            for k in range(H):
+                project(k)
+            inward(l, q)
+
+    def outward(l, q):
+        @pl.when(jnp.logical_not(is_hub))
+        def _():
+            index = jnp.where(here > hub - low, here - 1, here)
+            remote(
+                part.at[l, q, pl.ds(H, H)], far.at[l, q, index], o_send, o_recv.at[l, q], {"sp": hub}
+            ).start()
+
+    def inward(l, q):
+        for d, k in enumerate(near):
+            remote(
+                part.at[l, q, slot(k)], got.at[l, q, H - 2 - d], r_send, r_recv.at[l, q], {"sp": k}
+            ).start()
+
+    def stage_s(l, q):
+        with jax.named_scope(f"s{l}{q}"):
+
+            @pl.when(is_hub)
+            def _():
+                landed(far.at[l, q], o_recv.at[l, q])
+                for k in range(H):
+                    value = part[l, q, H + k].astype(F32)
+                    for d in range(H - 1):
+                        value = value + far[l, q, d, k].astype(F32)
+                    part[l, q, H + k] = value.astype(BF16)
+                    remote(
+                        part.at[l, q, H + k], got.at[l, q, H - 1], o_send, r_recv.at[l, q], {"sp": away[k]}
+                    ).start()
+
+    def ready(m):
+        landed(block(m, mate), wo_recv.at[m])
+        weight_last(m)
+
+    def stage_b(l, q):
+        with jax.named_scope(f"b{l}{q}"):
+            squares_wait(psq, l, q, rq_recv)
+            inverse = column(lax.rsqrt(total(psq, l, q) / width + EPS))
+            landed(got.at[l, q], r_recv.at[l, q])
+            value = part[l, q, here].astype(F32)
+            for k in range(H):
+                value = value + got[l, q, k].astype(F32)
+            ext[l, q, HALO:, :] = (value * wide(inverse, group)).astype(BF16)
+            if q + 1 < S:
+                halo_copy(l, q).start()
+            else:
+                pl.when(t + 1 < T)(lambda: halo_copy(l, q).start())
+
+    def halo_wait(l, q):
+        landed(ext.at[l, q, pl.ds(0, HALO), :], h_recv.at[l, q])
+
+    def stage_c(l, q):
+        with jax.named_scope(f"c{l}{q}"):
+            smooth(l, q)
+
+    def smooth(l, q):
+        if q == 0:
+            pl.when(t > 0)(lambda: halo_wait(l, q))
+
+            @pl.when(t == 0)
+            def _():
+                ext[l, q, pl.ds(0, HALO), :] = jnp.zeros((HALO, group), BF16)
+
+            pl.when(t != s)(lambda: landed(wp.at[l], p_recv.at[l]))
+            if l == 0:
+                pl.when(t != s)(lambda: landed(scales, c_recv))
+        else:
+            halo_wait(l, q)
+        values = ext[l, q].astype(F32)
+        reach = values
+        pooled = values
+        for k in range(S):
+            reach = reach + pltpu.roll(reach, 2**k, 0)
+            pooled = jnp.where(s == k, reach, pooled)
+        window = jnp.left_shift(2, s)
+        place = q * R + t * C + lax.broadcasted_iota(jnp.int32, (C, group), 0)
+        count = jnp.minimum(place + 1, window).astype(F32)
+        spread = (pooled[HALO:, :] / count - values[HALO:, :]).astype(BF16)
+        mixed = jnp.dot(spread, wp[l], preferred_element_type=F32)
+        mix[l, q, here] = (mixed * scales[l : l + 1, :]).astype(BF16)
+
+        def on(k, kind):
+            lower = lax.div(k, H) * H
+            remote(
+                mix.at[l, q, here], mix.at[l, q, lax.rem(s - lower + S, S)],
+                m_send.at[3 if kind else 0], m_recv.at[kind, l, q], {"sp": k},
+            ).start()
+
+        for k in near:
+            on(k, 0)
+        pl.when(is_hub)(lambda: on(far_hub, 1))
+
+    def mates_view(l, q):
+        return mix.at[l, q, pl.ds(0, H - 1)]
+
+    def stage_f(l, q):
+        with jax.named_scope(f"f{l}{q}"):
+
+            @pl.when(is_hub)
+            def _():
+                landed(mates_view(l, q), m_recv.at[0, l, q])
+                for j in range(1, H):
+                    from_here = lax.rem(here + j, H)
+                    for k in away:
+                        remote(
+                            mix.at[l, q, from_here], mix.at[l, q, H + from_here],
+                            m_send.at[1], m_recv.at[2, l, q], {"sp": k},
+                        ).start()
+
+    def stage_g(l, q):
+        with jax.named_scope(f"g{l}{q}"):
+
+            @pl.when(is_hub)
+            def _():
+                spot = slot(far_hub)
+                landed(mix.at[l, q, spot], m_recv.at[1, l, q])
+                for k in near:
+                    remote(
+                        mix.at[l, q, spot], mix.at[l, q, spot],
+                        m_send.at[2], m_recv.at[1, l, q], {"sp": k},
+                    ).start()
+
+    def stage_d(l, q):
+        with jax.named_scope(f"d{l}{q}"):
+            if q == 0:
+                ready(2 * l + 1)
+
+            @pl.when(jnp.logical_not(is_hub))
+            def _():
+                landed(mates_view(l, q), m_recv.at[0, l, q])
+                landed(mix.at[l, q, 0], m_recv.at[1, l, q])
+
+            landed(mates_view(l, q), m_recv.at[2, l, q])
+            value = jnp.dot(
+                jnp.concatenate([mix[l, q, k] for k in range(S)], axis=1), wout[l],
+                preferred_element_type=F32,
+            )
+            branch[q] = value
+            bsq[l, q, 0] = line(lanes(value * value))
+            squares_start(bsq, l, q, mq_send, mq_recv)
+
+    smalls[0].start()
+    for m in range(M):
+        load(m).start()
+    smalls[1].start()
+    smalls[2].start()
+    pool_load = [pltpu.make_async_copy(w_pool.at[l, 0], wp.at[l], p_recv.at[l]) for l in range(layers)]
+
+    @pl.when(t == s)
+    def _():
+        for l in range(layers):
+            pool_load[l].start()
+        scale_load.start()
+
+    smalls[0].wait()
+    pl.semaphore_wait(barrier, S * T - 1 + (1 if sides == 2 else 0))
+
+    for _, q in others:
+        run_copy(q * 2 + c, t).start()
+        run_copy(q * 2 + 1 - c, t).start()
+    run_copy(mate, t).start()
+    stream_on(t, True)
+    weight_own(0)
+    for h in range(PARTS):
+        weight_cross(0, h)
+    weight_own(1)
+    for h in range(PARTS):
+        weight_cross(1, h)
+    with jax.named_scope("enter"):
+        landed(rows_in.at[mate], y_recv.at[mate])
+        stream_on(mate)
+        for _, q in others:
+            for core in (c, 1 - c):
+                landed(rows_in.at[q * 2 + core], y_recv.at[q * 2 + core])
+                stream_on(q * 2 + core)
+
+    @pl.when(t == s)
+    def _():
+        for l in range(layers):
+            pool_load[l].wait()
+        scale_load.wait()
+        for d in range(1, T):
+            scale_copy(d).start()
+
+    pool_send(0)
+    smalls[1].wait()
+    smalls[2].wait()
+
+    actions = (
+        stage_a, stage_b, stage_c, stage_d, weight_own, pool_send, weight_cross, weight_relay, weight_second,
+        stage_s, stage_f, stage_g,
+    )
+    for kind, *where in order:
+        actions[kind](*where)
+
+    rows = pl.ds(0, (T - 1) * C)
+
+    @pl.when(s == t)
+    def _():
+        final_self(s).wait()
+        landed(out.at[rows, :], f_recv)
+        sent(out.at[rows, :], f_send)
+
+    @pl.when(s != t)
+    def _():
+        landed(out, f_recv)
+        sent(out, f_send)
+
+    with jax.named_scope("drain"):
+        sent(stream.at[rows, :], y_send)
+        sent(x.at[pl.ds(0, S - 1)], x_send)
+
+        @pl.when(t == s)
+        def _():
+            for d in range(1, T):
+                sent(scales, c_send.at[d - 1])
+                sent(wp, p_send.at[d - 1])
+
+        for m in range(M):
+            sent(block(m, t), wo_send.at[m])
+            for d, q in others:
+                sent(share(m, t), wx_send.at[m, d])
+                sent(block(m, t), wf_send.at[m, d])
+                if sides == 2:
+                    sent(share(m, t), wy_send.at[m, d])
+        sent(psq.at[:, :, pl.ds(0, S - 1)], rq_send)
+        sent(bsq.at[:, :, pl.ds(0, S - 1)], mq_send)
+        sent(part.at[:, :, pl.ds(0, H - 1)], r_send)
+        sent(part.at[:, :, pl.ds(0, H)], o_send)
+        sent(mix.at[:, :, pl.ds(0, H - 1)], m_send.at[0])
+
+        @pl.when(is_hub)
+        def _():
+            sent(mix.at[:, :, 0], m_send.at[3])
+            sent(mix.at[:, :, pl.ds(0, (H - 1) * H)], m_send.at[1])
+            sent(mix.at[:, :, pl.ds(0, H - 1)], m_send.at[2])
+
+        sent(ext.at[:, pl.ds(0, S - 1), pl.ds(0, HALO), :], h_send.at[0])
+        pl.when(t + 1 < T)(lambda: sent(ext.at[:, 0, pl.ds(0, HALO), :], h_send.at[1]))
+
+
+def stage_order(layers, runs):
+    steps = []
+    begins = {0: 0, 9: AT_S, 1: AT_B, 2: AT_C, 10: AT_F, 11: AT_G, 3: AT_D}
+    for l in range(layers + 1):
+        for kind, at in begins.items():
+            if l < layers or kind == 0:
+                for q in range(runs):
+                    steps.append((l * PERIOD + at + q * STRIDE, (kind, l, q)))
+    for m in range(1, 2 * layers):
+        due = m // 2 * PERIOD + (AT_D if m % 2 else 0) - 0.1
+        begin = due - LEAD
+        if m == 1:
+            begin = due - (PARTS - 1) * SPACE - RELAY - SECOND
+        for h in range(PARTS):
+            if m > 1:
+                if h == 0:
+                    steps.append((begin, (4, m)))
+                    if m % 2 == 0:
+                        steps.append((begin, (5, m // 2)))
+                steps.append((begin + h * SPACE, (6, m, h)))
+            steps.append((begin + h * SPACE + RELAY, (7, m, h)))
+            steps.append((begin + h * SPACE + RELAY + SECOND, (8, m, h)))
+    return [step for _, step in sorted(steps)]
+
+
+def per_plane(G, S, T, stream, gain_pre, w_in, w_pool, pool_scale, w_out, gain_post):
+    layers, width = gain_pre.shape
+    R, F = stream.shape
+    group = w_pool.shape[2]
+    C = R // T
+    H = S // 2
+    pairs = T // 2
+    M = 2 * layers
+    wide = max(128, C)
+    dma = pltpu.SemaphoreType.DMA
+    anywhere = pl.BlockSpec(memory_space=pl.ANY)
+    return pl.pallas_call(
+        functools.partial(plane_kernel, G, S, T, layers, width, stage_order(layers, S)),
+        out_shape=jax.ShapeDtypeStruct((R, F), BF16),
+        in_specs=[anywhere] * 7,
+        out_specs=pl.BlockSpec(memory_space=pltpu.VMEM),
+        scratch_shapes=[
+            pltpu.VMEM((R, F), BF16),
+            pltpu.VMEM((layers, width), F32),
+            pltpu.VMEM((layers, width), F32),
+            pltpu.VMEM((layers, T, F, group), BF16),
+            pltpu.VMEM((layers, T * group, F), BF16),
+            pltpu.VMEM((layers, group, group), BF16),
+            pltpu.VMEM((layers, group), F32),
+            pltpu.VMEM((T, C, F), BF16),
+            pltpu.VMEM((S, C, F), BF16),
+            pltpu.VMEM((layers, S, S, C, group), BF16),
+            pltpu.VMEM((layers, S, H, C, group), BF16),
+            pltpu.VMEM((layers, S, H - 1, H, C, group), BF16),
+            pltpu.VMEM((layers, S, S, 8, wide), F32),
+            pltpu.VMEM((layers, S, HALO + C, group), BF16),
+            pltpu.VMEM((layers, S, S, C, group), BF16),
+            pltpu.VMEM((S, C, F), F32),
+            pltpu.VMEM((layers, S, S, 8, wide), F32),
+            dma((M,)),
+            dma((4,)),
+            dma((2,)),
+            dma(()),
+            dma((T,)),
+            dma(()),
+            dma((S,)),
+            dma(()),
+            dma(()),
+            dma((M,)),
+            dma((M,)),
+            dma((M, pairs - 1)),
+            dma((M, pairs - 1, PARTS)),
+            dma((M, pairs - 1)),
+            dma((M, pairs - 1, PARTS)),
+            dma((M, pairs - 1)),
+            dma((M, pairs - 1)),
+            dma((T - 1,)),
+            dma((layers,)),
+            dma((T - 1,)),
+            dma(()),
+            dma(()),
+            dma((layers, S)),
+            dma(()),
+            dma((layers, S)),
+            dma(()),
+            dma((layers, S)),
+            dma((2,)),
+            dma((layers, S)),
+            dma((4,)),
+            dma((3, layers, S)),
+            dma(()),
+            dma((layers, S)),
+        ],
+        compiler_params=pltpu.CompilerParams(
+            collective_id=0, has_side_effects=True, vmem_limit_bytes=60 * 1024 * 1024
+        ),
+    )(stream, gain_pre, w_in, w_pool, pool_scale, w_out, gain_post)
+
+
+def plan(G, S, T, *args):
+    stream, w_pool = args[0], args[3]
+    planes = S == T == T * w_pool.shape[1] and 2 < S and 2**S <= HALO and S % 2 == 0 and stream.shape[0] % (HALO * T) == 0
+    return (per_plane if planes else per_device)(G, S, T, *args)
+
+
 def solution(mesh):
     G, S, T = mesh.shape["grp"], mesh.shape["sp"], mesh.shape["tp"]
     return jax.shard_map(
-        functools.partial(per_device, G, S, T),
+        functools.partial(plan, G, S, T),
         mesh=mesh,
         in_specs=(
             P(("grp", "sp"), "tp"),

time: 146 us -> 115 us (0.79); the launches traced: 143 us -> 115 us
  Pallas kernels: 141 us -> 113 us
    pallas_call x1, Pallas kernels: 141 us -> 113 us  [per_plane(): pl.pallas_call(functools.partial(plane_kernel, G, S, T, layers, width, st...]
where the time goes in v1:
time: 115 us
  Pallas kernels  113 us (98%)
  local copies, waits for them, and re-layouts  1.87 us (2%)
    pallas_call x1, Pallas kernels, per_plane(): pl.pallas_call(functools.partial(plane_kernel, G, S, T, layers, width, st...  113 us

profile of v1, /device:TPU:25, one launch (start us, length us, event | category | flops | bytes accessed | tf_op | source)
XLA Modules:
  0.0 115.3 jit_solution(8515401917475878828)
XLA Ops:
  0.0 113.4 %shard_map.73 = bf16[256,1024]{1,0:T(8,128)(2,1)} custom-call(bf16[256,1024]{1,0:T(8,128)(2,1)} %stream_hbm.1, f32[3,4096]{1,0:T(4,128)} %gain_pre_hbm.1, bf16[3,1024,256]{2,1,0:T(8,128)(2,1)} %w_in.1, bf16[3,1,256,256]{3,2,1,0:T(8,128)(2,1)} %w_pool.1, f32[3,256]{1,0:T(4,128)} %scale_hbm.1, bf16[3,256,1024]{2,1,0:T(8,128)(2,1)} %w_out.1, ...), custom_call_target="tpu_custom_call" | custom-call | tf_op jit(solution)/shard_map/pallas_call | solution.py:1004
  113.4 1.9 %copy.9 = bf16[256,1024]{1,0:T(8,128)(2,1)} copy(bf16[256,1024]{1,0:T(8,128)(2,1)} %shard_map.73) | data formatting | bytes 1048576

commit v2 on v1

--- a/solution.py
+++ b/solution.py
@@ -12,9 +12,12 @@
 CHUNKS = 4
 PIECES = 2
 PARTS = 4
-PERIOD, STRIDE = 18, 2
-AT_S, AT_B, AT_C, AT_F, AT_G, AT_D = 2.6, 6, 8, 10.3, 10.8, 13.5
-LEAD, SPACE, RELAY, SECOND = 17.9, 1.5, 8, 4
+RELAYED = True
+OUT_SPEC = pl.BlockSpec(memory_space=pl.ANY)
+PERIOD, STRIDES = 17, (2, 2.5, 2.5)
+AT_S, AT_B, AT_F, AT_G, AT_D, AT_Z = 3, 6.2, 9.6, 9.7, 13, 0
+EARLY = (1.5, 0.75)
+SPACE, LEADS, RELAYS, SECONDS, FIRST = 1.5, (16.9, 16.9), (8, 8), (4, 4), (8, 4)
 MESH = pl.DeviceIdType.MESH
 F32 = jnp.float32
 BF16 = jnp.bfloat16
@@ -474,12 +477,12 @@
     G, S, T, layers, width, order,
     stream_hbm, gain_pre_hbm, w_in, w_pool, scale_hbm, w_out, gain_post_hbm,
     out,
-    stream, gain_pre, gain_post, win, wout, wp, scales, rows_in, x,
-    part, got, far, psq, ext, mix, branch, bsq,
+    stream, gain_pre, gain_post, win, wout, wp, scales, rows_in, x, held,
+    part, got, far, edge, psq, esq, mix, branch, bsq,
     load_sem, small_sem, self_sem, y_send, y_recv, x_send, x_recv, f_send, f_recv,
     wo_send, wo_recv, wx_send, wx_recv, wy_send, wy_recv, wf_send, wf_recv,
     p_send, p_recv, c_send, c_recv,
-    r_send, r_recv, o_send, o_recv, rq_send, rq_recv, h_send, h_recv, m_send, m_recv, mq_send, mq_recv,
+    r_send, r_recv, o_send, o_recv, rq_send, rq_recv, h_send, h_recv, hq_send, hq_recv, m_send, m_recv, mq_send, mq_recv,
 ):
     g, s, t = lax.axis_index("grp"), lax.axis_index("sp"), lax.axis_index("tp")
     pairs = T // 2
@@ -622,28 +625,46 @@
         row = jnp.sum(jnp.transpose(square), axis=0, keepdims=True)
         return jnp.broadcast_to(row, (8, line_width))
 
-    def column(values):
-        return jnp.transpose(jnp.concatenate([values] * 16, axis=0))[:C]
+    def column(values, first=0):
+        return jnp.transpose(jnp.concatenate([values] * 16, axis=0))[first:C]
 
     def wide(values, n):
         return jnp.concatenate([values] * (n // 128), axis=1)
 
     def squares_start(ref, l, q, send, recv):
         for d in range(1, S):
-            remote(ref.at[l, q, 0], ref.at[l, q, d], send, recv.at[l, q], {"sp": lax.rem(s + d, S)}).start()
+            remote(ref.at[l, q, 0], ref.at[l, q, d], send, recv.at[q], {"sp": lax.rem(s + d, S)}).start()
 
     def squares_wait(ref, l, q, recv):
-        landed(ref.at[l, q, pl.ds(1, S - 1)], recv.at[l, q])
+        landed(ref.at[l, q, pl.ds(1, S - 1)], recv.at[q])
 
     def total(ref, l, q):
         return sum(ref[l, q, k] for k in range(S))
 
-    def halo_copy(l, q):
-        ahead = q + lax.div(t + 1, T)
-        return remote(
-            ext.at[l, q, pl.ds(C, HALO), :], ext.at[l, ahead, pl.ds(0, HALO), :],
-            h_send.at[1 if q + 1 == S else 0], h_recv.at[l, ahead], {"tp": lax.rem(t + 1, T)},
-        )
+    def next_run(l, q, start):
+        if q + 1 < S:
+            start(q + lax.div(t + 1, T), 0)
+        else:
+            pl.when(t + 1 < T)(lambda: start(q, 1))
+
+    def edge_copy(l, q, k, index, plane, final):
+        def start(ahead, last):
+            remote(
+                part.at[l, q, k, pl.ds(C - HALO, HALO), :], edge.at[l, ahead, index],
+                h_send.at[2 * final + last], h_recv.at[l, ahead], {"sp": plane, "tp": lax.rem(t + 1, T)},
+            ).start()
+
+        next_run(l, q, start)
+
+    def edge_squares(l, q):
+        def start(ahead, last):
+            for d in range(S):
+                remote(
+                    psq.at[l, q, 0], esq.at[l, ahead, d], hq_send.at[last], hq_recv.at[l, ahead],
+                    {"sp": lax.rem(s + d, S), "tp": lax.rem(t + 1, T)},
+                ).start()
+
+        next_run(l, q, start)
 
     def run_copy(to, origin):
         rows = pl.ds(pl.multiple_of(to * C, 16), C)
@@ -688,71 +709,76 @@
             new = new.astype(BF16)
             x[q] = new
             if l == layers:
-                mine = jnp.logical_and(s == q, t == s)
-                pl.when(mine)(lambda: final_self(q).start())
-                pl.when(jnp.logical_not(mine))(lambda: final_copy(q).start())
                 return
             value = new.astype(F32)
-        psq[l, q, 0] = line(lanes(value * value))
-        squares_start(psq, l, q, rq_send, rq_recv)
         scaled = (value * features(gain_pre, l)).astype(BF16)
-
-        def project(k):
-            part[l, q, k] = jnp.dot(scaled, win[l, k], preferred_element_type=F32).astype(BF16)
-
-        if q == 0 and l == 0:
-            project(slot(t))
-            landed(block(0, mate), wo_recv.at[0])
-            project(slot(mate))
-            for h in range(PARTS):
-                weight_relay(0, h)
-            for h in range(PARTS):
-                weight_second(0, h)
-            for _, d in others:
-                project(slot(d * 2 + c))
-            weight_last(0)
-            for _, d in others:
-                project(slot(d * 2 + 1 - c))
-            outward(l, q)
-            inward(l, q)
+        if l == 0:
+            held[q] = scaled
+            pl.when(p == low // H)(lambda: inward(l, q, scaled))
+            pl.when(p != low // H)(lambda: outward(l, q, scaled))
         else:
             if q == 0:
                 ready(2 * l)
-            for k in range(H, S):
-                project(k)
-            outward(l, q)
-            for k in range(H):
-                project(k)
-            inward(l, q)
-
-    def outward(l, q):
+            outward(l, q, scaled)
+        psq[l, q, 0] = line(lanes(value * value))
+        squares_start(psq, l, q, rq_send, rq_recv)
+        edge_squares(l, q)
+        if l > 0:
+            inward(l, q, scaled)
+
+    def stage_e(q):
+        with jax.named_scope(f"e{q}"):
+            pl.when(p == low // H)(lambda: outward(0, q, held[q]))
+            pl.when(p != low // H)(lambda: inward(0, q, held[q]))
+
+    def weight_first():
+        with jax.named_scope("first"):
+            weight_last(0)
+
+    def stage_z(q):
+        mine = jnp.logical_and(s == q, t == s)
+        pl.when(mine)(lambda: final_self(q).start())
+        pl.when(jnp.logical_not(mine))(lambda: final_copy(q).start())
+
+    def project(l, q, k, scaled):
+        part[l, q, k] = jnp.dot(scaled, win[l, k], preferred_element_type=F32).astype(BF16)
+
+    def outward(l, q, scaled):
+        for k in range(H, S):
+            project(l, q, k, scaled)
+
         @pl.when(jnp.logical_not(is_hub))
         def _():
             index = jnp.where(here > hub - low, here - 1, here)
             remote(
-                part.at[l, q, pl.ds(H, H)], far.at[l, q, index], o_send, o_recv.at[l, q], {"sp": hub}
+                part.at[l, q, pl.ds(H, H)], far.at[l, q, index], o_send, o_recv.at[q], {"sp": hub}
             ).start()
 
-    def inward(l, q):
+    def inward(l, q, scaled):
+        for k in range(H):
+            project(l, q, k, scaled)
         for d, k in enumerate(near):
             remote(
-                part.at[l, q, slot(k)], got.at[l, q, H - 2 - d], r_send, r_recv.at[l, q], {"sp": k}
+                part.at[l, q, slot(k)], got.at[l, q, H - 2 - d], r_send, r_recv.at[q], {"sp": k}
             ).start()
+            edge_copy(l, q, slot(k), H - 2 - d, k, 0)
+        edge_copy(l, q, here, H, s, 0)
 
     def stage_s(l, q):
         with jax.named_scope(f"s{l}{q}"):
 
             @pl.when(is_hub)
             def _():
-                landed(far.at[l, q], o_recv.at[l, q])
+                landed(far.at[l, q], o_recv.at[q])
                 for k in range(H):
                     value = part[l, q, H + k].astype(F32)
                     for d in range(H - 1):
                         value = value + far[l, q, d, k].astype(F32)
                     part[l, q, H + k] = value.astype(BF16)
                     remote(
-                        part.at[l, q, H + k], got.at[l, q, H - 1], o_send, r_recv.at[l, q], {"sp": away[k]}
+                        part.at[l, q, H + k], got.at[l, q, H - 1], o_send, r_recv.at[q], {"sp": away[k]}
                     ).start()
+                    edge_copy(l, q, H + k, H - 1, away[k], 1)
 
     def ready(m):
         landed(block(m, mate), wo_recv.at[m])
@@ -760,39 +786,31 @@
 
     def stage_b(l, q):
         with jax.named_scope(f"b{l}{q}"):
-            squares_wait(psq, l, q, rq_recv)
-            inverse = column(lax.rsqrt(total(psq, l, q) / width + EPS))
-            landed(got.at[l, q], r_recv.at[l, q])
-            value = part[l, q, here].astype(F32)
-            for k in range(H):
-                value = value + got[l, q, k].astype(F32)
-            ext[l, q, HALO:, :] = (value * wide(inverse, group)).astype(BF16)
-            if q + 1 < S:
-                halo_copy(l, q).start()
-            else:
-                pl.when(t + 1 < T)(lambda: halo_copy(l, q).start())
-
-    def halo_wait(l, q):
-        landed(ext.at[l, q, pl.ds(0, HALO), :], h_recv.at[l, q])
-
-    def stage_c(l, q):
-        with jax.named_scope(f"c{l}{q}"):
             smooth(l, q)
 
     def smooth(l, q):
+        squares_wait(psq, l, q, rq_recv)
+        inverse = column(lax.rsqrt(total(psq, l, q) / width + EPS))
+
+        def arrived():
+            landed(esq.at[l, q], hq_recv.at[l, q])
+            landed(edge.at[l, q], h_recv.at[l, q])
+
         if q == 0:
-            pl.when(t > 0)(lambda: halo_wait(l, q))
-
-            @pl.when(t == 0)
-            def _():
-                ext[l, q, pl.ds(0, HALO), :] = jnp.zeros((HALO, group), BF16)
-
+            pl.when(t > 0)(arrived)
             pl.when(t != s)(lambda: landed(wp.at[l], p_recv.at[l]))
             if l == 0:
                 pl.when(t != s)(lambda: landed(scales, c_recv))
         else:
-            halo_wait(l, q)
-        values = ext[l, q].astype(F32)
+            arrived()
+        before = column(lax.rsqrt(total(esq, l, q) / width + EPS), C - HALO)
+        ahead = sum(edge[l, q, k].astype(F32) for k in range(H + 1))
+        landed(got.at[l, q], r_recv.at[q])
+        value = part[l, q, here].astype(F32)
+        for k in range(H):
+            value = value + got[l, q, k].astype(F32)
+        values = jnp.concatenate([ahead * wide(before, group), value * wide(inverse, group)], axis=0)
+        values = values.astype(BF16).astype(F32)
         reach = values
         pooled = values
         for k in range(S):
@@ -809,12 +827,13 @@
             lower = lax.div(k, H) * H
             remote(
                 mix.at[l, q, here], mix.at[l, q, lax.rem(s - lower + S, S)],
-                m_send.at[3 if kind else 0], m_recv.at[kind, l, q], {"sp": k},
+                m_send.at[3 if kind else 0], m_recv.at[kind, q], {"sp": k},
             ).start()
 
-        for k in near:
+        for k in near if RELAYED else planes:
             on(k, 0)
-        pl.when(is_hub)(lambda: on(far_hub, 1))
+        if RELAYED:
+            pl.when(is_hub)(lambda: on(far_hub, 1))
 
     def mates_view(l, q):
         return mix.at[l, q, pl.ds(0, H - 1)]
@@ -824,13 +843,13 @@
 
             @pl.when(is_hub)
             def _():
-                landed(mates_view(l, q), m_recv.at[0, l, q])
+                landed(mates_view(l, q), m_recv.at[0, q])
                 for j in range(1, H):
                     from_here = lax.rem(here + j, H)
                     for k in away:
                         remote(
                             mix.at[l, q, from_here], mix.at[l, q, H + from_here],
-                            m_send.at[1], m_recv.at[2, l, q], {"sp": k},
+                            m_send.at[1], m_recv.at[2, q], {"sp": k},
                         ).start()
 
     def stage_g(l, q):
@@ -839,11 +858,11 @@
             @pl.when(is_hub)
             def _():
                 spot = slot(far_hub)
-                landed(mix.at[l, q, spot], m_recv.at[1, l, q])
+                landed(mix.at[l, q, spot], m_recv.at[1, q])
                 for k in near:
                     remote(
                         mix.at[l, q, spot], mix.at[l, q, spot],
-                        m_send.at[2], m_recv.at[1, l, q], {"sp": k},
+                        m_send.at[2], m_recv.at[1, q], {"sp": k},
                     ).start()
 
     def stage_d(l, q):
@@ -851,12 +870,16 @@
             if q == 0:
                 ready(2 * l + 1)
 
-            @pl.when(jnp.logical_not(is_hub))
-            def _():
-                landed(mates_view(l, q), m_recv.at[0, l, q])
-                landed(mix.at[l, q, 0], m_recv.at[1, l, q])
-
-            landed(mates_view(l, q), m_recv.at[2, l, q])
+            if RELAYED:
+
+                @pl.when(jnp.logical_not(is_hub))
+                def _():
+                    landed(mates_view(l, q), m_recv.at[0, q])
+                    landed(mix.at[l, q, 0], m_recv.at[1, q])
+
+                landed(mates_view(l, q), m_recv.at[2, q])
+            else:
+                landed(mix.at[l, q, pl.ds(0, S - 1)], m_recv.at[0, q])
             value = jnp.dot(
                 jnp.concatenate([mix[l, q, k] for k in range(S)], axis=1), wout[l],
                 preferred_element_type=F32,
@@ -877,6 +900,12 @@
         for l in range(layers):
             pool_load[l].start()
         scale_load.start()
+
+    @pl.when(t == 0)
+    def _():
+        for l in range(layers):
+            edge[l, 0] = jnp.zeros(edge.shape[2:], BF16)
+            esq[l, 0] = jnp.zeros(esq.shape[2:], F32)
 
     smalls[0].wait()
     pl.semaphore_wait(barrier, S * T - 1 + (1 if sides == 2 else 0))
@@ -899,6 +928,9 @@
             for core in (c, 1 - c):
                 landed(rows_in.at[q * 2 + core], y_recv.at[q * 2 + core])
                 stream_on(q * 2 + core)
+        for h in range(PARTS):
+            weight_relay(0, h)
+    landed(block(0, mate), wo_recv.at[0])
 
     @pl.when(t == s)
     def _():
@@ -913,8 +945,8 @@
     smalls[2].wait()
 
     actions = (
-        stage_a, stage_b, stage_c, stage_d, weight_own, pool_send, weight_cross, weight_relay, weight_second,
-        stage_s, stage_f, stage_g,
+        stage_a, stage_b, None, stage_d, weight_own, pool_send, weight_cross, weight_relay, weight_second,
+        stage_s, stage_f, stage_g, stage_z, stage_e, weight_first,
     )
     for kind, *where in order:
         actions[kind](*where)
@@ -953,31 +985,55 @@
         sent(bsq.at[:, :, pl.ds(0, S - 1)], mq_send)
         sent(part.at[:, :, pl.ds(0, H - 1)], r_send)
         sent(part.at[:, :, pl.ds(0, H)], o_send)
-        sent(mix.at[:, :, pl.ds(0, H - 1)], m_send.at[0])
-
-        @pl.when(is_hub)
+        sent(mix.at[:, :, pl.ds(0, (H if RELAYED else S) - 1)], m_send.at[0])
+
+        @pl.when(is_hub if RELAYED else s < 0)
         def _():
             sent(mix.at[:, :, 0], m_send.at[3])
             sent(mix.at[:, :, pl.ds(0, (H - 1) * H)], m_send.at[1])
             sent(mix.at[:, :, pl.ds(0, H - 1)], m_send.at[2])
 
-        sent(ext.at[:, pl.ds(0, S - 1), pl.ds(0, HALO), :], h_send.at[0])
-        pl.when(t + 1 < T)(lambda: sent(ext.at[:, 0, pl.ds(0, HALO), :], h_send.at[1]))
+        sent(edge.at[:, pl.ds(0, S - 1), pl.ds(0, H)], h_send.at[0])
+        sent(esq.at[:, pl.ds(0, S - 1)], hq_send.at[0])
+        pl.when(is_hub)(lambda: sent(edge.at[:, pl.ds(0, S - 1), pl.ds(0, H)], h_send.at[2]))
+
+        @pl.when(t + 1 < T)
+        def _():
+            sent(edge.at[:, 0, pl.ds(0, H)], h_send.at[1])
+            sent(esq.at[:, 0], hq_send.at[1])
+            pl.when(is_hub)(lambda: sent(edge.at[:, 0, pl.ds(0, H)], h_send.at[3]))
 
 
 def stage_order(layers, runs):
     steps = []
-    begins = {0: 0, 9: AT_S, 1: AT_B, 2: AT_C, 10: AT_F, 11: AT_G, 3: AT_D}
+    begins = {0: 0, 9: AT_S, 1: AT_B, 3: AT_D}
+    if RELAYED:
+        begins |= {10: AT_F, 11: AT_G}
+    steps.append((-90, (14,)))
+    for h in range(PARTS):
+        steps.append((-100 + EARLY[0] + h * EARLY[1], (8, 0, h)))
     for l in range(layers + 1):
         for kind, at in begins.items():
             if l < layers or kind == 0:
                 for q in range(runs):
-                    steps.append((l * PERIOD + at + q * STRIDE, (kind, l, q)))
+                    pace = STRIDES[0 if l == 0 else 1 if l + 1 < layers else 2]
+                    if l == 0 and kind == 0:
+                        steps.append((q - 100, (0, 0, q)))
+                        steps.append((q * pace, (13, q)))
+                    else:
+                        steps.append((l * PERIOD + at + q * pace, (kind, l, q)))
+    last = max(at for at, step in steps if step[0] == 3)
+    for at, step in list(steps):
+        if step[:2] == (0, layers):
+            steps.append((max(at, last + AT_Z) + 0.01, (12, step[2])))
     for m in range(1, 2 * layers):
         due = m // 2 * PERIOD + (AT_D if m % 2 else 0) - 0.1
-        begin = due - LEAD
+        odd = m % 2
+        begin = due - LEADS[odd]
+        relay, second = RELAYS[odd], SECONDS[odd]
         if m == 1:
-            begin = due - (PARTS - 1) * SPACE - RELAY - SECOND
+            relay, second = FIRST
+            begin = due - (PARTS - 1) * SPACE - relay - second
         for h in range(PARTS):
             if m > 1:
                 if h == 0:
@@ -985,8 +1041,8 @@
                     if m % 2 == 0:
                         steps.append((begin, (5, m // 2)))
                 steps.append((begin + h * SPACE, (6, m, h)))
-            steps.append((begin + h * SPACE + RELAY, (7, m, h)))
-            steps.append((begin + h * SPACE + RELAY + SECOND, (8, m, h)))
+            steps.append((begin + h * SPACE + relay, (7, m, h)))
+            steps.append((begin + h * SPACE + relay + second, (8, m, h)))
     return [step for _, step in sorted(steps)]
 
 
@@ -1005,7 +1061,7 @@
         functools.partial(plane_kernel, G, S, T, layers, width, stage_order(layers, S)),
         out_shape=jax.ShapeDtypeStruct((R, F), BF16),
         in_specs=[anywhere] * 7,
-        out_specs=pl.BlockSpec(memory_space=pltpu.VMEM),
+        out_specs=OUT_SPEC,
         scratch_shapes=[
             pltpu.VMEM((R, F), BF16),
             pltpu.VMEM((layers, width), F32),
@@ -1016,11 +1072,13 @@
             pltpu.VMEM((layers, group), F32),
             pltpu.VMEM((T, C, F), BF16),
             pltpu.VMEM((S, C, F), BF16),
+            pltpu.VMEM((S, C, F), BF16),
             pltpu.VMEM((layers, S, S, C, group), BF16),
             pltpu.VMEM((layers, S, H, C, group), BF16),
             pltpu.VMEM((layers, S, H - 1, H, C, group), BF16),
+            pltpu.VMEM((layers, S, H + 1, HALO, group), BF16),
             pltpu.VMEM((layers, S, S, 8, wide), F32),
-            pltpu.VMEM((layers, S, HALO + C, group), BF16),
+            pltpu.VMEM((layers, S, S, 8, wide), F32),
             pltpu.VMEM((layers, S, S, C, group), BF16),
             pltpu.VMEM((S, C, F), F32),
             pltpu.VMEM((layers, S, S, 8, wide), F32),
@@ -1046,17 +1104,19 @@
             dma((T - 1,)),
             dma(()),
             dma(()),
-            dma((layers, S)),
+            dma((S,)),
             dma(()),
-            dma((layers, S)),
+            dma((S,)),
             dma(()),
+            dma((S,)),
+            dma((4,)),
             dma((layers, S)),
             dma((2,)),
             dma((layers, S)),
             dma((4,)),
-            dma((3, layers, S)),
+            dma((3, S)),
             dma(()),
-            dma((layers, S)),
+            dma((S,)),
         ],
         compiler_params=pltpu.CompilerParams(
             collective_id=0, has_side_effects=True, vmem_limit_bytes=60 * 1024 * 1024
@@ -1066,7 +1126,7 @@
 
 def plan(G, S, T, *args):
     stream, w_pool = args[0], args[3]
-    planes = S == T == T * w_pool.shape[1] and 2 < S and 2**S <= HALO and S % 2 == 0 and stream.shape[0] % (HALO * T) == 0
+    planes = S == T == T * w_pool.shape[1] and S // 2 == T // 2 == 2 and stream.shape[0] % (HALO * T) == 0
     return (per_plane if planes else per_device)(G, S, T, *args)
 
 

time: 115 us -> 108 us (0.939)
  Pallas kernels: 113 us -> 106 us
    pallas_call x1, Pallas kernels: 113 us -> 106 us  [per_plane(): pl.pallas_call(functools.partial(plane_kernel, G, S, T, layers, width, st...]
where the time goes in v2:
time: 108 us
  Pallas kernels  106 us (98%)
  local copies, waits for them, and re-layouts  1.87 us (2%)
    pallas_call x1, Pallas kernels, per_plane(): pl.pallas_call(functools.partial(plane_kernel, G, S, T, layers, width, st...  106 us

profile of v2, /device:TPU:25, one launch (start us, length us, event | category | flops | bytes accessed | tf_op | source)
XLA Modules:
  0.0 107.6 jit_solution(6372735015816830977)
XLA Ops:
  0.0 105.7 %shard_map.73 = bf16[256,1024]{1,0:T(8,128)(2,1)} custom-call(bf16[256,1024]{1,0:T(8,128)(2,1)} %stream_hbm.1, f32[3,4096]{1,0:T(4,128)} %gain_pre_hbm.1, bf16[3,1024,256]{2,1,0:T(8,128)(2,1)} %w_in.1, bf16[3,1,256,256]{3,2,1,0:T(8,128)(2,1)} %w_pool.1, f32[3,256]{1,0:T(4,128)} %scale_hbm.1, bf16[3,256,1024]{2,1,0:T(8,128)(2,1)} %w_out.1, ...), custom_call_target="tpu_custom_call" | custom-call | tf_op jit(solution)/shard_map/pallas_call | solution.py:1060
  105.7 1.9 %copy.9 = bf16[256,1024]{1,0:T(8,128)(2,1)} copy(bf16[256,1024]{1,0:T(8,128)(2,1)} %shard_map.73) | data formatting | bytes 1048576

commit v3 on v2

--- a/solution.py
+++ b/solution.py
@@ -15,9 +15,10 @@
 RELAYED = True
 OUT_SPEC = pl.BlockSpec(memory_space=pl.ANY)
 PERIOD, STRIDES = 17, (2, 2.5, 2.5)
-AT_S, AT_B, AT_F, AT_G, AT_D, AT_Z = 3, 6.2, 9.6, 9.7, 13, 0
+AT_S, AT_B, AT_F, AT_G, AT_D, AT_Z = 2.3, 5.6, 9.6, 9.7, 13, 0
+CUTS = 2
 EARLY = (1.5, 0.75)
-SPACE, LEADS, RELAYS, SECONDS, FIRST = 1.5, (16.9, 16.9), (8, 8), (4, 4), (8, 4)
+SPACE, LEADS, RELAYS, SECONDS, FIRST = 1.3, (16.9, 16.9), (9, 8), (3.4, 4), (8, 4)
 MESH = pl.DeviceIdType.MESH
 F32 = jnp.float32
 BF16 = jnp.bfloat16
@@ -502,6 +503,7 @@
     is_hub = s == hub
     near = [low + lax.rem(here + d, H) for d in range(1, H)]
     away = [H - low + d for d in range(H)]
+    spread_order = [jnp.where(low == 0, H - 1 - d, d) for d in range(H)]
     planes = near + away
 
     def slot(k):
@@ -666,21 +668,30 @@
 
         next_run(l, q, start)
 
-    def run_copy(to, origin):
-        rows = pl.ds(pl.multiple_of(to * C, 16), C)
-        return remote(stream.at[rows, :], rows_in.at[origin], y_send, y_recv.at[origin], {"tp": to})
-
-    def run_of(f, local):
-        return stream.at[pl.ds(pl.multiple_of(t * C, 16), C), :] if local else rows_in.at[f]
-
-    def stream_self(local):
-        return pltpu.make_async_copy(run_of(s, local), x.at[s], self_sem.at[0])
-
-    def stream_on(f, local=False):
-        pl.when(f == s)(lambda: stream_self(local).start())
-        pl.when(f != s)(
-            lambda: remote(run_of(f, local), x.at[s], x_send, x_recv.at[s], {"sp": f}).start()
+    step = C // CUTS
+
+    def run_copy(to, origin, n):
+        rows = pl.ds(pl.multiple_of(to * C + n * step, 16), step)
+        return remote(
+            stream.at[rows, :], rows_in.at[origin, pl.ds(n * step, step)],
+            y_send, y_recv.at[origin, n], {"tp": to},
         )
+
+    def run_landed(origin, n):
+        landed(rows_in.at[origin, pl.ds(n * step, step)], y_recv.at[origin, n])
+
+    def run_of(f, n, local):
+        if local:
+            return stream.at[pl.ds(pl.multiple_of(t * C + n * step, 16), step), :]
+        return rows_in.at[f, pl.ds(n * step, step)]
+
+    def stream_on(f, n, local=False):
+        view = x.at[s, pl.ds(n * step, step)]
+        pl.when(f == s)(lambda: pltpu.make_async_copy(run_of(f, n, local), view, self_sem.at[0]).start())
+        pl.when(f != s)(lambda: remote(run_of(f, n, local), view, x_send, x_recv.at[s], {"sp": f}).start())
+
+    def stream_self_wait():
+        pltpu.make_async_copy(rows_in.at[s], x.at[s], self_sem.at[0]).wait()
 
     def final_copy(q):
         rows = pl.ds(pl.multiple_of(t * C, 16), C)
@@ -699,7 +710,7 @@
 
     def advance(l, q):
         if l == 0:
-            pl.when(s == q)(lambda: stream_self(False).wait())
+            pl.when(s == q)(stream_self_wait)
             pl.when(s != q)(lambda: landed(x.at[q], x_recv.at[q]))
             value = x[q].astype(F32)
         else:
@@ -744,15 +755,14 @@
         part[l, q, k] = jnp.dot(scaled, win[l, k], preferred_element_type=F32).astype(BF16)
 
     def outward(l, q, scaled):
-        for k in range(H, S):
-            project(l, q, k, scaled)
-
-        @pl.when(jnp.logical_not(is_hub))
-        def _():
-            index = jnp.where(here > hub - low, here - 1, here)
-            remote(
-                part.at[l, q, pl.ds(H, H)], far.at[l, q, index], o_send, o_recv.at[q], {"sp": hub}
-            ).start()
+        index = jnp.where(here > hub - low, here - 1, here)
+        for j, k in enumerate(spread_order):
+            project(l, q, H + k, scaled)
+            pl.when(jnp.logical_not(is_hub))(
+                lambda j=j, k=k: remote(
+                    part.at[l, q, H + k], far.at[l, q, index, k], o_send, o_recv.at[j, q], {"sp": hub}
+                ).start()
+            )
 
     def inward(l, q, scaled):
         for k in range(H):
@@ -769,16 +779,16 @@
 
             @pl.when(is_hub)
             def _():
-                landed(far.at[l, q], o_recv.at[q])
-                for k in range(H):
+                for j, k in enumerate(spread_order):
+                    landed(far.at[l, q, pl.ds(0, H - 1), k], o_recv.at[j, q])
                     value = part[l, q, H + k].astype(F32)
                     for d in range(H - 1):
                         value = value + far[l, q, d, k].astype(F32)
                     part[l, q, H + k] = value.astype(BF16)
                     remote(
-                        part.at[l, q, H + k], got.at[l, q, H - 1], o_send, r_recv.at[q], {"sp": away[k]}
+                        part.at[l, q, H + k], got.at[l, q, H - 1], o_send, r_recv.at[q], {"sp": H - low + k}
                     ).start()
-                    edge_copy(l, q, H + k, H - 1, away[k], 1)
+                    edge_copy(l, q, H + k, H - 1, H - low + k, 1)
 
     def ready(m):
         landed(block(m, mate), wo_recv.at[m])
@@ -846,7 +856,7 @@
                 landed(mates_view(l, q), m_recv.at[0, q])
                 for j in range(1, H):
                     from_here = lax.rem(here + j, H)
-                    for k in away:
+                    for k in [H - low + d for d in spread_order]:
                         remote(
                             mix.at[l, q, from_here], mix.at[l, q, H + from_here],
                             m_send.at[1], m_recv.at[2, q], {"sp": k},
@@ -910,11 +920,13 @@
     smalls[0].wait()
     pl.semaphore_wait(barrier, S * T - 1 + (1 if sides == 2 else 0))
 
-    for _, q in others:
-        run_copy(q * 2 + c, t).start()
-        run_copy(q * 2 + 1 - c, t).start()
-    run_copy(mate, t).start()
-    stream_on(t, True)
+    for n in range(CUTS):
+        for _, q in others:
+            run_copy(q * 2 + c, t, n).start()
+            run_copy(q * 2 + 1 - c, t, n).start()
+    for n in range(CUTS):
+        run_copy(mate, t, n).start()
+        stream_on(t, n, True)
     weight_own(0)
     for h in range(PARTS):
         weight_cross(0, h)
@@ -922,12 +934,14 @@
     for h in range(PARTS):
         weight_cross(1, h)
     with jax.named_scope("enter"):
-        landed(rows_in.at[mate], y_recv.at[mate])
-        stream_on(mate)
-        for _, q in others:
-            for core in (c, 1 - c):
-                landed(rows_in.at[q * 2 + core], y_recv.at[q * 2 + core])
-                stream_on(q * 2 + core)
+        for n in range(CUTS):
+            run_landed(mate, n)
+            stream_on(mate, n)
+        for n in range(CUTS):
+            for _, q in others:
+                for core in (c, 1 - c):
+                    run_landed(q * 2 + core, n)
+                    stream_on(q * 2 + core, n)
         for h in range(PARTS):
             weight_relay(0, h)
     landed(block(0, mate), wo_recv.at[0])
@@ -1086,7 +1100,7 @@
             dma((4,)),
             dma((2,)),
             dma(()),
-            dma((T,)),
+            dma((T, CUTS)),
             dma(()),
             dma((S,)),
             dma(()),
@@ -1106,7 +1120,7 @@
             dma(()),
             dma((S,)),
             dma(()),
-            dma((S,)),
+            dma((H, S)),
             dma(()),
             dma((S,)),
             dma((4,)),
@@ -1126,7 +1140,7 @@
 
 def plan(G, S, T, *args):
     stream, w_pool = args[0], args[3]
-    planes = S == T == T * w_pool.shape[1] and S // 2 == T // 2 == 2 and stream.shape[0] % (HALO * T) == 0
+    planes = S == T == T * w_pool.shape[1] and S // 2 == T // 2 == 2 and stream.shape[0] % (HALO * CUTS * T) == 0
     return (per_plane if planes else per_device)(G, S, T, *args)
 
 

time: 108 us -> 107 us (level)
    pallas_call x1, Pallas kernels: 106 us -> 105 us  [per_plane(): pl.pallas_call(functools.partial(plane_kernel, G, S, T, layers, width, st...]
where the time goes in v3:
time: 107 us; the launch traced here: 106 us
  Pallas kernels  105 us (98%)
  local copies, waits for them, and re-layouts  1.87 us (2%)
    pallas_call x1, Pallas kernels, per_plane(): pl.pallas_call(functools.partial(plane_kernel, G, S, T, layers, width, st...  105 us

profile of v3, /device:TPU:25, one launch (start us, length us, event | category | flops | bytes accessed | tf_op | source)
XLA Modules:
  0.0 106.4 jit_solution(6884236519240440028)
XLA Ops:
  0.0 104.5 %shard_map.73 = bf16[256,1024]{1,0:T(8,128)(2,1)} custom-call(bf16[256,1024]{1,0:T(8,128)(2,1)} %stream_hbm.1, f32[3,4096]{1,0:T(4,128)} %gain_pre_hbm.1, bf16[3,1024,256]{2,1,0:T(8,128)(2,1)} %w_in.1, bf16[3,1,256,256]{3,2,1,0:T(8,128)(2,1)} %w_pool.1, f32[3,256]{1,0:T(4,128)} %scale_hbm.1, bf16[3,256,1024]{2,1,0:T(8,128)(2,1)} %w_out.1, ...), custom_call_target="tpu_custom_call" | custom-call | tf_op jit(solution)/shard_map/pallas_call | solution.py:1074
  104.5 1.9 %copy.9 = bf16[256,1024]{1,0:T(8,128)(2,1)} copy(bf16[256,1024]{1,0:T(8,128)(2,1)} %shard_map.73) | data formatting | bytes 1048576
